TPU v7x, 32 devices: a whole 2x2x4 slice. The times are simulated.
32 devices in a mesh: sp: 8 (over z, x), tp: 4 (over y, core).
Axes of the slice: x: 2, y: 2, z: 4, core: 2. Of those that a mesh axis runs over, the one named last changes fastest.
Arguments:
- query_proj: bfloat16 [4096, 1024], P('sp', 'tp'), may hold values from -6 to 6
- projected_keys: bfloat16 [4096, 512], P('sp', 'tp'), may hold values from -6 to 6
- projected_values: bfloat16 [4096, 512], P('sp', 'tp'), may hold values from -6 to 6
- residual: bfloat16 [4096, 2048], P(('sp', 'tp')), may hold values from -6 to 6
- out_weight: bfloat16 [1024, 2048], replicated, may hold values from -0.1875 to 0.1875
- mix_gain: float32 [2048], replicated, may hold values from 0.1 to 1.9
- norm_gain: float32 [2048], replicated, may hold values from 0.1 to 1.9
- route_expert: int32 [4096, 2], P(('sp', 'tp')), may hold values from 0 to 31, all different within a row; in each aligned block of 128 rows (0 to 127, 128 to 255, ...) at most 16 rows name the same one
- route_weight: float32 [4096, 2], P(('sp', 'tp')), may hold values from 0.2 to 1
- expert_gate: bfloat16 [32, 2048, 1024], P(('sp', 'tp')), may hold values from -0.125 to 0.125
- expert_up: bfloat16 [32, 2048, 1024], P(('sp', 'tp')), may hold values from -0.125 to 0.125
- expert_down: bfloat16 [32, 1024, 2048], P(('sp', 'tp')), may hold values from -0.1875 to 0.1875
Outputs:
- output: bfloat16 [4096, 2048], P(('sp', 'tp'))
Inputs may be any that keep to these rules, and one draw needn't show every extreme that they name: `route_expert`: each row names 2 different experts. The rows of one device (aligned blocks of 128 rows) name any one expert at most 16 times, and in some blocks some expert is named exactly 16 times.
All inputs are finite; a program needn't handle non-finite values.
Results may differ from a plain program's by a relative error of at most 0.015.
Values may be sent and summed in bfloat16 or wider, within the bound.
A program may use at most 128 MiB of HBM per device.

v0:
```python
import math
import jax
import jax.numpy as jnp
from jax import lax
from jax.sharding import PartitionSpec as P

D = 2048
HEAD_SIZE = 64
GRID_W = 64
epsilon = 1e-06
base_theta = 10000.0


def unit_length_rows(values):
    values = values.astype(jnp.float32)
    return values * lax.rsqrt(jnp.mean(values * values, axis=-1, keepdims=True) + epsilon)


def rotary_embed(head_vecs, offset):
    row_count = head_vecs.shape[0]
    quarter = head_vecs.shape[-1] // 4
    places = offset + jnp.arange(row_count, dtype=jnp.int32)
    grid_row = (places // GRID_W).astype(jnp.float32)
    grid_col = (places % GRID_W).astype(jnp.float32)
    frequency = base_theta ** (-jnp.arange(quarter, dtype=jnp.float32) / quarter)
    row_angle = grid_row[:, None, None] * frequency
    col_angle = grid_col[:, None, None] * frequency
    row_cos, row_sin = (jnp.cos(row_angle), jnp.sin(row_angle))
    col_cos, col_sin = (jnp.cos(col_angle), jnp.sin(col_angle))
    row_first = head_vecs[..., :quarter]
    row_second = head_vecs[..., quarter : 2 * quarter]
    col_first = head_vecs[..., 2 * quarter : 3 * quarter]
    col_second = head_vecs[..., 3 * quarter :]
    return jnp.concatenate(
        [
            row_first * row_cos - row_second * row_sin,
            row_second * row_cos + row_first * row_sin,
            col_first * col_cos - col_second * col_sin,
            col_second * col_cos + col_first * col_sin,
        ],
        axis=-1,
    )


def local(
    query_proj,
    projected_keys,
    projected_values,
    residual,
    out_weight,
    mix_gain,
    norm_gain,
    route_expert,
    route_weight,
    expert_gate,
    expert_up,
    expert_down,
):
    tok_count = query_proj.shape[0]
    q_heads = query_proj.shape[1] // HEAD_SIZE
    kv_heads = projected_keys.shape[1] // HEAD_SIZE
    query_group = q_heads // kv_heads
    offset = lax.axis_index("sp") * tok_count
    query_prepared = rotary_embed(
        unit_length_rows(query_proj.reshape(tok_count, q_heads, HEAD_SIZE)), offset
    ).astype(jnp.bfloat16)
    query_prepared = query_prepared.reshape(tok_count, kv_heads, query_group, HEAD_SIZE)
    key_prepared = rotary_embed(
        unit_length_rows(projected_keys.reshape(tok_count, kv_heads, HEAD_SIZE)), offset
    ).astype(jnp.bfloat16)
    v_ready = projected_values.reshape(tok_count, kv_heads, HEAD_SIZE)
    scale = HEAD_SIZE ** (-0.5)
    sums_start = jnp.zeros((tok_count, kv_heads, query_group, HEAD_SIZE), jnp.float32)
    totals_start = jnp.zeros((tok_count, kv_heads, query_group), jnp.float32)
    keys_all = lax.all_gather(key_prepared, "sp", axis=0, tiled=True)
    vals_all = lax.all_gather(v_ready, "sp", axis=0, tiled=True)
    key_count = keys_all.shape[0]
    model_width = math.gcd(key_count, 1024)
    key_blocks = keys_all.reshape(key_count // model_width, model_width, kv_heads, HEAD_SIZE)
    val_blocks = vals_all.reshape(key_count // model_width, model_width, kv_heads, HEAD_SIZE)

    def one_block(inner, pair):
        sums, totals = inner
        scores = (
            jnp.einsum(
                "thgd,nhd->thgn", query_prepared, pair[0], preferred_element_type=jnp.float32
            )
            * scale
        )
        weights = jnp.exp(scores)
        totals = totals + jnp.sum(weights, axis=-1)
        sums = sums + jnp.einsum(
            "thgn,nhd->thgd",
            weights.astype(jnp.bfloat16),
            pair[1],
            preferred_element_type=jnp.float32,
        )
        return ((sums, totals), None)

    result, unused = lax.scan(one_block, (sums_start, totals_start), (key_blocks, val_blocks))
    sums, totals = result
    attended = (
        (sums / totals[..., None]).astype(jnp.bfloat16).reshape(tok_count, q_heads * HEAD_SIZE)
    )
    by_token = lax.all_to_all(attended, "tp", split_axis=0, concat_axis=1, tiled=True)
    mixed = jnp.dot(by_token, out_weight, preferred_element_type=jnp.float32)
    stream = (residual.astype(jnp.float32) + unit_length_rows(mixed) * mix_gain).astype(
        jnp.bfloat16
    )
    normed = (unit_length_rows(stream) * norm_gain).astype(jnp.bfloat16)
    row_count = normed.shape[0]
    top_count = route_expert.shape[1]
    experts = lax.axis_size("sp") * lax.axis_size("tp")
    capacity = max(2, 2 * top_count * row_count // experts)
    flat_expert = route_expert.reshape(-1)
    onehot = (flat_expert[:, None] == jnp.arange(experts, dtype=jnp.int32)[None, :]).astype(
        jnp.int32
    )
    earlier = jnp.cumsum(onehot, axis=0) - onehot
    slot_rank = jnp.sum(earlier * onehot, axis=1)
    target = flat_expert * capacity + slot_rank
    placing = jnp.arange(experts * capacity, dtype=jnp.int32)[:, None] == target[None, :]
    placing = jnp.any(placing.reshape(experts * capacity, row_count, top_count), axis=2).astype(
        jnp.bfloat16
    )
    outgoing = jnp.dot(placing, normed, preferred_element_type=jnp.float32).astype(jnp.bfloat16)
    outgoing = outgoing.reshape(experts, capacity, D)
    gate_mat = expert_gate[0]
    up_mat = expert_up[0]
    down_mat = expert_down[0]
    slots = lax.all_to_all(outgoing, ("sp", "tp"), split_axis=0, concat_axis=0, tiled=True)
    flat_rows = slots.reshape(-1, slots.shape[-1])
    gate_pre = jnp.dot(flat_rows, gate_mat, preferred_element_type=jnp.float32)
    up_pre = jnp.dot(flat_rows, up_mat, preferred_element_type=jnp.float32)
    expert_act = (jax.nn.silu(gate_pre) * up_pre).astype(jnp.bfloat16)
    done = jnp.dot(expert_act, down_mat, preferred_element_type=jnp.float32).astype(jnp.bfloat16)
    answered = done.reshape(slots.shape)
    returned = lax.all_to_all(answered, ("sp", "tp"), split_axis=0, concat_axis=0, tiled=True)
    picked = jnp.take(returned.reshape(experts * capacity, D), target, axis=0).reshape(
        row_count, top_count, D
    )
    combined = jnp.sum(picked.astype(jnp.float32) * route_weight[:, :, None], axis=1)
    return (stream.astype(jnp.float32) + combined).astype(jnp.bfloat16)


def solution(mesh):
    return jax.shard_map(
        local,
        mesh=mesh,
        in_specs=(
            P("sp", "tp"),
            P("sp", "tp"),
            P("sp", "tp"),
            P(("sp", "tp"), None),
            P(),
            P(),
            P(),
            P(("sp", "tp"), None),
            P(("sp", "tp"), None),
            P(("sp", "tp"), None, None),
            P(("sp", "tp"), None, None),
            P(("sp", "tp"), None, None),
        ),
        out_specs=P(("sp", "tp"), None),
        check_vma=False,
    )
```

profile of v0, /device:TPU:0, one launch (start us, length us, event | category | flops | bytes accessed | tf_op | source)
XLA Modules:
  0.0 279.2 jit_solution(4073406177149737743)
XLA Ops:
  8.8 1.7 copy.71
  14.1 37.4 %all-gather.5.cloned.1.call-done = bf16[4096,2,64]{0,2,1:T(8,128)(2,1)} async-done(((bf16[512,2,64]{0,2,1:T(8,128)(2,1)}), bf16[4096,2,64]{0,2,1:T(8,128)(2,1)}) %all-gather.5.cloned.1.call-update) | async-done | bytes 1048592 | tf_op jit(solution)/shard_map/all_gather | solution.py:75
  51.5 1.3 copy.93
  52.8 39.2 %all-gather.3.cloned.1.call-done = bf16[4096,2,64]{0,2,1:T(8,128)(2,1)} async-done(((bf16[512,2,64]{0,2,1:T(8,128)(2,1)}), bf16[4096,2,64]{0,2,1:T(8,128)(2,1)}) %all-gather.3.cloned.1.call-update) | async-done | bytes 1048592 | tf_op jit(solution)/shard_map/all_gather | solution.py:76
  93.3 38.0 %while.13 = (s32[]{:T(128)}, f32[512,2,2,64]{0,3,2,1:T(8,128)S(1)}, f32[512,2,2]{0,2,1:T(2,128)S(1)}, bf16[4,1024,2,64]{1,3,2,0:T(8,128)(2,1)S(1)}, bf16[4,1024,...) while((s32[]{:T(128)}, f32[512,2,2,64]{0,3,2,1:T(8,128)S(1)}, ...), condition=%wide.region_4.5_spmd.clone, body=%wide.region_2.4_spmd.clone.sunk | while | flops 545523712 | bytes 18645096 | solution.py:100
  93.4 4.6 %bitcast_reduce_fusion.2 = (f32[512,2,2]{0,2,1:T(2,128)S(1)}, f32[2,1024,512,2]{2,1,3,0:T(8,128)}) fusion(bf16[512,2,2,64]{0,3,2,1:T(8,128)(2,1)S(1)} %get-tuple-element.193, bf16[4,1024,2,64]{1,3,2,0:T(8,128)(2,1)S(1)} %get-tuple-element.192, s32[]{:T(128)} %get-tuple-element.180), kind=kOutput, calls=%fused_computation.1.clone.1 | convolution fusion | flops 272627712 | bytes 8921092 | tf_op jit(solution)/shard_map/while/body/eval_jaxpr/thgd,nhd->thgn/dot_general | solution.py:85
  98.0 4.9 %fusion.58 = f32[512,2,2,64]{0,3,2,1:T(8,128)S(1)} fusion(f32[2,1024,512,2]{2,1,3,0:T(8,128)} %get-tuple-element.170, f32[512,2,2,64]{0,3,2,1:T(8,128)S(1)} %get-tuple-element.181, bf16[4,1024,2,64]{1,3,2,0:T(8,128)(2,1)S(1)} %get-tuple-element.191, s32[]{:T(128)} %get-tuple-element.180, pred[]{:T(512)S(6)} %compare.14), kind=kOutput, calls=%fused_computation.7.clone.1 | convolution fusion | flops 272891904 | bytes 9699333 | tf_op jit(solution)/shard_map/while/body/eval_jaxpr/thgn,nhd->thgd/dot_general | solution.py:92
  102.9 4.6 %bitcast_reduce_fusion.2 = (f32[512,2,2]{0,2,1:T(2,128)S(1)}, f32[2,1024,512,2]{2,1,3,0:T(8,128)}) fusion(bf16[512,2,2,64]{0,3,2,1:T(8,128)(2,1)S(1)} %get-tuple-element.193, bf16[4,1024,2,64]{1,3,2,0:T(8,128)(2,1)S(1)} %get-tuple-element.192, s32[]{:T(128)} %get-tuple-element.180), kind=kOutput, calls=%fused_computation.1.clone.1 | convolution fusion | flops 272627712 | bytes 8921092 | tf_op jit(solution)/shard_map/while/body/eval_jaxpr/thgd,nhd->thgn/dot_general | solution.py:85
  107.5 4.9 %fusion.58 = f32[512,2,2,64]{0,3,2,1:T(8,128)S(1)} fusion(f32[2,1024,512,2]{2,1,3,0:T(8,128)} %get-tuple-element.170, f32[512,2,2,64]{0,3,2,1:T(8,128)S(1)} %get-tuple-element.181, bf16[4,1024,2,64]{1,3,2,0:T(8,128)(2,1)S(1)} %get-tuple-element.191, s32[]{:T(128)} %get-tuple-element.180, pred[]{:T(512)S(6)} %compare.14), kind=kOutput, calls=%fused_computation.7.clone.1 | convolution fusion | flops 272891904 | bytes 9699333 | tf_op jit(solution)/shard_map/while/body/eval_jaxpr/thgn,nhd->thgd/dot_general | solution.py:92
  112.4 4.6 %bitcast_reduce_fusion.2 = (f32[512,2,2]{0,2,1:T(2,128)S(1)}, f32[2,1024,512,2]{2,1,3,0:T(8,128)}) fusion(bf16[512,2,2,64]{0,3,2,1:T(8,128)(2,1)S(1)} %get-tuple-element.193, bf16[4,1024,2,64]{1,3,2,0:T(8,128)(2,1)S(1)} %get-tuple-element.192, s32[]{:T(128)} %get-tuple-element.180), kind=kOutput, calls=%fused_computation.1.clone.1 | convolution fusion | flops 272627712 | bytes 8921092 | tf_op jit(solution)/shard_map/while/body/eval_jaxpr/thgd,nhd->thgn/dot_general | solution.py:85
  117.0 4.9 %fusion.58 = f32[512,2,2,64]{0,3,2,1:T(8,128)S(1)} fusion(f32[2,1024,512,2]{2,1,3,0:T(8,128)} %get-tuple-element.170, f32[512,2,2,64]{0,3,2,1:T(8,128)S(1)} %get-tuple-element.181, bf16[4,1024,2,64]{1,3,2,0:T(8,128)(2,1)S(1)} %get-tuple-element.191, s32[]{:T(128)} %get-tuple-element.180, pred[]{:T(512)S(6)} %compare.14), kind=kOutput, calls=%fused_computation.7.clone.1 | convolution fusion | flops 272891904 | bytes 9699333 | tf_op jit(solution)/shard_map/while/body/eval_jaxpr/thgn,nhd->thgd/dot_general | solution.py:92
  121.9 4.6 %bitcast_reduce_fusion.2 = (f32[512,2,2]{0,2,1:T(2,128)S(1)}, f32[2,1024,512,2]{2,1,3,0:T(8,128)}) fusion(bf16[512,2,2,64]{0,3,2,1:T(8,128)(2,1)S(1)} %get-tuple-element.193, bf16[4,1024,2,64]{1,3,2,0:T(8,128)(2,1)S(1)} %get-tuple-element.192, s32[]{:T(128)} %get-tuple-element.180), kind=kOutput, calls=%fused_computation.1.clone.1 | convolution fusion | flops 272627712 | bytes 8921092 | tf_op jit(solution)/shard_map/while/body/eval_jaxpr/thgd,nhd->thgn/dot_general | solution.py:85
  126.5 4.9 %fusion.58 = f32[512,2,2,64]{0,3,2,1:T(8,128)S(1)} fusion(f32[2,1024,512,2]{2,1,3,0:T(8,128)} %get-tuple-element.170, f32[512,2,2,64]{0,3,2,1:T(8,128)S(1)} %get-tuple-element.181, bf16[4,1024,2,64]{1,3,2,0:T(8,128)(2,1)S(1)} %get-tuple-element.191, s32[]{:T(128)} %get-tuple-element.180, pred[]{:T(512)S(6)} %compare.14), kind=kOutput, calls=%fused_computation.7.clone.1 | convolution fusion | flops 272891904 | bytes 9699333 | tf_op jit(solution)/shard_map/while/body/eval_jaxpr/thgn,nhd->thgd/dot_general | solution.py:92
  132.3 3.5 %all-to-all-start = ((bf16[4,128,256]{1,2,0:T(8,128)(2,1)}), bf16[4,128,256]{1,2,0:T(8,128)(2,1)S(1)}, u32[]{:S(2)}, u32[]{:S(2)}) async-start(bf16[4,128,256]{1,2,0:T(8,128)(2,1)} %copy.76), calls=%async_computation | async-start | bytes 524288 | tf_op jit(solution)/shard_map/all_to_all | solution.py:105
  135.9 5.9 %all-to-all-done = bf16[4,128,256]{1,2,0:T(8,128)(2,1)S(1)} async-done(((bf16[4,128,256]{1,2,0:T(8,128)(2,1)}), bf16[4,128,256]{1,2,0:T(8,128)(2,1)S(1)}, u32[]{:S(2)}, u32[]{:S(2)}) %all-to-all-start) | async-done | bytes 262176 | tf_op jit(solution)/shard_map/all_to_all | solution.py:105
  141.8 3.0 %multiply_reduce_fusion.1 = (f32[128]{0:T(128)S(1)}, f32[128,2048]{1,0:T(8,128)S(1)}) fusion(bf16[128,1024]{0,1:T(8,128)(2,1)S(1)} %bitcast.119, bf16[1024,2048]{1,0:T(8,128)(2,1)} %param.18), kind=kOutput, calls=%fused_computation.38 | convolution fusion | flops 537395072 | bytes 5505536 | tf_op jit(solution)/shard_map/dot_general | solution.py:106
  146.0 51.2 %all_to_all.29 = bf16[32,16,2048]{2,1,0:T(8,128)(2,1)S(1)} all-to-all(bf16[32,16,2048]{2,1,0:T(8,128)(2,1)S(1)} %bitcast.113), channel_id=1, replica_groups=mesh['sp'=8,'tp'=4] {'sp','tp'}, dimensions={0} | all-to-all | bytes 4194304 | tf_op jit(solution)/shard_map/all_to_all | solution.py:131
  197.2 3.7 %fusion.16 = f32[512,1024]{1,0:T(8,128)} fusion(bf16[512,2048]{1,0:T(8,128)(2,1)S(1)} %bitcast.117, bf16[1,2048,1024]{2,1,0:T(8,128)(2,1)S(1)} %copy-done.5), kind=kOutput, calls=%fused_computation.21 | convolution fusion | flops 2147483648 | bytes 8388608 | tf_op jit(solution)/shard_map/dot_general | solution.py:133
  200.9 9.9 %fusion.18 = bf16[512,2048]{1,0:T(8,128)(2,1)} fusion(bf16[1,1024,2048]{2,1,0:T(8,128)(2,1)} %param.25, f32[512,1024]{1,0:T(8,128)} %fusion.16, bf16[512,2048]{1,0:T(8,128)(2,1)S(1)} %bitcast.118, bf16[1,2048,1024]{2,1,0:T(8,128)(2,1)} %param.24), kind=kOutput, calls=%fused_computation.23 | convolution fusion | flops 4299161600 | bytes 14680064 | tf_op jit(solution)/shard_map/dot_general | solution.py:136
  210.8 3.7 %all-to-all-start.2 = ((bf16[32,16,2048]{2,1,0:T(8,128)(2,1)}), bf16[32,16,2048]{2,1,0:T(8,128)(2,1)S(1)}, u32[]{:S(2)}, u32[]{:S(2)}) async-start(bf16[32,16,2048]{2,1,0:T(8,128)(2,1)} %bitcast.116), calls=%async_computation.2 | async-start | bytes 4194304 | tf_op jit(solution)/shard_map/all_to_all | solution.py:138
  215.1 48.2 %all-to-all-done.2 = bf16[32,16,2048]{2,1,0:T(8,128)(2,1)S(1)} async-done(((bf16[32,16,2048]{2,1,0:T(8,128)(2,1)}), bf16[32,16,2048]{2,1,0:T(8,128)(2,1)S(1)}, u32[]{:S(2)}, u32[]{:S(2)}) %all-to-all-start.2) | async-done | bytes 2097184 | tf_op jit(solution)/shard_map/all_to_all | solution.py:138
  263.2 2.3 gather_fusion
  265.6 1.7 gather.7
  267.3 4.1 %multiply_reduce_fusion = f32[128,2048]{1,0:T(8,128)S(1)} fusion(bf16[128,2,2048]{2,1,0:T(2,128)(2,1)S(1)} %gather.7, pred[128,2]{1,0:T(8,128)(4,1)S(1)} %copy.81, f32[128,2]{1,0:T(8,128)S(1)} %copy.83), kind=kLoop, calls=%fused_computation.25 | loop fusion | flops 1835008 | bytes 2098432 | tf_op jit(solution)/shard_map/reduce_sum | solution.py:142
  (66 shorter events, 10.7 us)
Async XLA Ops:
  6.5 45.0 %all-gather.5.cloned.1.call-start = ((), (), s32[]{:S(2)}) async-start(), calls=%async_computation.4 | async-start | bytes 1179648 | tf_op jit(solution)/shard_map/all_gather | solution.py:75
  8.7 83.3 %all-gather.3.cloned.1.call-start = ((), (), s32[]{:S(2)}) async-start(), calls=%async_computation.3 | async-start | bytes 1179648 | tf_op jit(solution)/shard_map/all_gather | solution.py:76
  93.3 42.5 %copy-start.1 = (s32[128,2]{0,1:T(2,128)S(1)}, s32[128,2]{0,1:T(2,128)}, u32[]{:S(2)}) copy-start(s32[128,2]{0,1:T(2,128)} %param.21) | copy-start | bytes 3076
  131.4 13.4 %copy-start = (bf16[128,2048]{1,0:T(8,128)(2,1)S(1)}, bf16[128,2048]{1,0:T(8,128)(2,1)}, u32[]{:S(2)}) copy-start(bf16[128,2048]{1,0:T(8,128)(2,1)} %param.17) | copy-start | bytes 1572868
  131.4 13.4 %copy-start.2 = (f32[2048]{0:T(1024)S(1)}, f32[2048]{0:T(1024)}, u32[]{:S(2)}) copy-start(f32[2048]{0:T(1024)} %param.19) | copy-start | bytes 24580
  132.3 13.0 %copy-start.3 = (f32[2048]{0:T(1024)S(1)}, f32[2048]{0:T(1024)}, u32[]{:S(2)}) copy-start(f32[2048]{0:T(1024)} %param.20) | copy-start | bytes 24580
  132.3 9.5 %all-to-all-start = ((bf16[4,128,256]{1,2,0:T(8,128)(2,1)}), bf16[4,128,256]{1,2,0:T(8,128)(2,1)S(1)}, u32[]{:S(2)}, u32[]{:S(2)}) async-start(bf16[4,128,256]{1,2,0:T(8,128)(2,1)} %copy.76), calls=%async_computation | async-start | bytes 524288 | tf_op jit(solution)/shard_map/all_to_all | solution.py:105
  144.8 52.4 %copy-start.5 = (bf16[1,2048,1024]{2,1,0:T(8,128)(2,1)S(1)}, bf16[1,2048,1024]{2,1,0:T(8,128)(2,1)}, u32[]{:S(2)}) copy-start(bf16[1,2048,1024]{2,1,0:T(8,128)(2,1)} %param.23) | copy-start | bytes 12582916
  210.8 4.1 %copy-start.4 = (f32[128,2]{0,1:T(2,128)S(1)}, f32[128,2]{0,1:T(2,128)}, u32[]{:S(2)}) copy-start(f32[128,2]{0,1:T(2,128)} %param.22) | copy-start | bytes 3076
  210.8 52.4 %all-to-all-start.2 = ((bf16[32,16,2048]{2,1,0:T(8,128)(2,1)}), bf16[32,16,2048]{2,1,0:T(8,128)(2,1)S(1)}, u32[]{:S(2)}, u32[]{:S(2)}) async-start(bf16[32,16,2048]{2,1,0:T(8,128)(2,1)} %bitcast.116), calls=%async_computation.2 | async-start | bytes 4194304 | tf_op jit(solution)/shard_map/all_to_all | solution.py:138
Sparse Core Ops, SparseCore 0:
  9.4 42.1 all-gather.4
  53.6 38.3 all-gather.2
where the time goes:
time: 280 us; the launch traced here: 279 us
  waiting for transfers between devices  131 us (47%)
  matrix products  55.3 us (20%)
  blocking collectives  51.2 us (18%)
  between operations  13.7 us (5%)
  local copies, waits for them, and re-layouts  13.3 us (5%)
  other arithmetic  7.73 us (3%)
  starting transfers between devices  7.26 us (3%)
    all_to_all x1, blocking collectives, local(): lax.all_to_all(outgoing, ('sp', 'tp'), split_axis=0, concat_axis=0, tiled...  51.2 us
    all_to_all x1, waiting for transfers between devices, local(): lax.all_to_all(answered, ('sp', 'tp'), split_axis=0, concat_axis=0, tiled...  48.2 us
    all_gather x1, waiting for transfers between devices, local(): vals_all = lax.all_gather(v_ready, 'sp', axis=0, tiled=True)  39.2 us
    all_gather x1, waiting for transfers between devices, local(): keys_all = lax.all_gather(key_prepared, 'sp', axis=0, tiled=True)  37.4 us
    dot_general x4, matrix products, one_block(): jnp.einsum('thgn,nhd->thgd', weights.astype(jnp.bfloat16), pair[1], prefe...  19.4 us
    dot_general x4, matrix products, one_block(): jnp.einsum('thgd,nhd->thgn', query_prepared, pair[0], preferred_element_t...  18.4 us
    dot_general x1, matrix products, local(): jnp.dot(expert_act, down_mat, preferred_element_type=jnp.float32)  9.89 us
    all_to_all x1, waiting for transfers between devices, local(): lax.all_to_all(attended, 'tp', split_axis=0, concat_axis=1, tiled=True)  5.88 us
  transfers between devices with their start and end apart: 4, of which 4 were waited for; matrix products, arithmetic and copies ran while one was open for 3% of the time, Pallas kernels for 0%

commit v1 on v0

--- a/solution.py
+++ b/solution.py
@@ -72,7 +72,13 @@
     scale = HEAD_SIZE ** (-0.5)
     sums_start = jnp.zeros((tok_count, kv_heads, query_group, HEAD_SIZE), jnp.float32)
     totals_start = jnp.zeros((tok_count, kv_heads, query_group), jnp.float32)
-    keys_all = lax.all_gather(key_prepared, "sp", axis=0, tiled=True)
+    size = lax.axis_size("sp")
+    moving, blocks = (key_prepared, [key_prepared])
+    for _ in range(size - 1):
+        moving = lax.ppermute(moving, "sp", [(i, (i + 1) % size) for i in range(size)])
+        blocks.insert(0, moving)
+    row_of_blocks = jnp.concatenate(blocks, axis=0)
+    keys_all = jnp.roll(row_of_blocks, (lax.axis_index("sp") + 1) * key_prepared.shape[0], axis=0)
     vals_all = lax.all_gather(v_ready, "sp", axis=0, tiled=True)
     key_count = keys_all.shape[0]
     model_width = math.gcd(key_count, 1024)

time: 280 us -> 255 us (0.911)
  waiting for transfers between devices: 131 us -> 106 us
  starting transfers between devices: 7.26 us -> 10.5 us
    ppermute x0 -> x7, waiting for transfers between devices: none -> 51.7 us  [local(): lax.ppermute(moving, 'sp', [(i, (i + 1) % size) for i in range(size)])]
    all_gather x1, waiting for transfers between devices: 39.2 us -> 0.02 us  [local(): vals_all = lax.all_gather(v_ready, 'sp', axis=0, tiled=True)]
    all_gather x1 -> x0, waiting for transfers between devices: 37.4 us -> none  [local(): keys_all = lax.all_gather(key_prepared, 'sp', axis=0, tiled=True)]
    ppermute x0 -> x7, starting transfers between devices: none -> 3.49 us  [local(): lax.ppermute(moving, 'sp', [(i, (i + 1) % size) for i in range(size)])]
  transfers between devices with their start and end apart: 4 -> 10, of which waited for: 4 -> 9; matrix products, arithmetic and copies ran while one was open for 3% -> 2% of each run, Pallas kernels for 0% -> 0%
where the time goes in v1:
time: 255 us; the launch traced here: 254 us
  waiting for transfers between devices  106 us (42%)
  matrix products  55.3 us (22%)
  blocking collectives  50.7 us (20%)
  between operations  13.9 us (5%)
  local copies, waits for them, and re-layouts  10.9 us (4%)
  starting transfers between devices  10.5 us (4%)
  other arithmetic  7.08 us (3%)
    ppermute x7, waiting for transfers between devices, local(): lax.ppermute(moving, 'sp', [(i, (i + 1) % size) for i in range(size)])  51.7 us
    all_to_all x1, blocking collectives, local(): lax.all_to_all(outgoing, ('sp', 'tp'), split_axis=0, concat_axis=0, tiled...  50.7 us
    all_to_all x1, waiting for transfers between devices, local(): lax.all_to_all(answered, ('sp', 'tp'), split_axis=0, concat_axis=0, tiled...  48.2 us
    dot_general x4, matrix products, one_block(): jnp.einsum('thgn,nhd->thgd', weights.astype(jnp.bfloat16), pair[1], prefe...  19.4 us
    dot_general x4, matrix products, one_block(): jnp.einsum('thgd,nhd->thgn', query_prepared, pair[0], preferred_element_t...  18.4 us
    dot_general x1, matrix products, local(): jnp.dot(expert_act, down_mat, preferred_element_type=jnp.float32)  9.89 us
    all_to_all x1, waiting for transfers between devices, local(): lax.all_to_all(attended, 'tp', split_axis=0, concat_axis=1, tiled=True)  5.89 us
  transfers between devices with their start and end apart: 10, of which 9 were waited for; matrix products, arithmetic and copies ran while one was open for 2% of the time, Pallas kernels for 0%

profile of v1, /device:TPU:0, one launch (start us, length us, event | category | flops | bytes accessed | tf_op | source)
XLA Modules:
  0.0 254.3 jit_solution(6639145262729813667)
XLA Ops:
  13.1 4.6 %collective-permute-done = bf16[512,2,64]{0,2,1:T(8,128)(2,1)S(1)} collective-permute-done((bf16[512,2,64]{0,2,1:T(8,128)(2,1)S(1)}, bf16[512,2,64]{0,2,1:T(8,128)(2,1)S(1)}, u32[]{:S(2)}, u32[]{:S(2)}) %collective-permute-start) | collective-permute-done | bytes 131104 | tf_op jit(solution)/shard_map/ppermute | solution.py:78
  18.3 7.2 %collective-permute-done.1 = bf16[512,2,64]{0,2,1:T(8,128)(2,1)S(1)} collective-permute-done((bf16[512,2,64]{0,2,1:T(8,128)(2,1)S(1)}, bf16[512,2,64]{0,2,1:T(8,128)(2,1)S(1)}, u32[]{:S(2)}, u32[]{:S(2)}) %collective-permute-start.1) | collective-permute-done | bytes 131104 | tf_op jit(solution)/shard_map/ppermute | solution.py:78
  26.0 7.8 %collective-permute-done.2 = bf16[512,2,64]{0,2,1:T(8,128)(2,1)S(1)} collective-permute-done((bf16[512,2,64]{0,2,1:T(8,128)(2,1)S(1)}, bf16[512,2,64]{0,2,1:T(8,128)(2,1)S(1)}, u32[]{:S(2)}, u32[]{:S(2)}) %collective-permute-start.2) | collective-permute-done | bytes 131104 | tf_op jit(solution)/shard_map/ppermute | solution.py:78
  33.8 7.6 %collective-permute-done.3 = bf16[512,2,64]{0,2,1:T(8,128)(2,1)S(1)} collective-permute-done((bf16[512,2,64]{0,2,1:T(8,128)(2,1)S(1)}, bf16[512,2,64]{0,2,1:T(8,128)(2,1)S(1)}, u32[]{:S(2)}, u32[]{:S(2)}) %collective-permute-start.3) | collective-permute-done | bytes 131104 | tf_op jit(solution)/shard_map/ppermute | solution.py:78
  41.5 8.1 %collective-permute-done.4 = bf16[512,2,64]{0,2,1:T(8,128)(2,1)S(1)} collective-permute-done((bf16[512,2,64]{0,2,1:T(8,128)(2,1)S(1)}, bf16[512,2,64]{0,2,1:T(8,128)(2,1)S(1)}, u32[]{:S(2)}, u32[]{:S(2)}) %collective-permute-start.4) | collective-permute-done | bytes 131104 | tf_op jit(solution)/shard_map/ppermute | solution.py:78
  50.2 9.2 %collective-permute-done.5 = bf16[512,2,64]{0,2,1:T(8,128)(2,1)S(1)} collective-permute-done((bf16[512,2,64]{0,2,1:T(8,128)(2,1)S(1)}, bf16[512,2,64]{0,2,1:T(8,128)(2,1)S(1)}, u32[]{:S(2)}, u32[]{:S(2)}) %collective-permute-start.5) | collective-permute-done | bytes 131104 | tf_op jit(solution)/shard_map/ppermute | solution.py:78
  59.7 7.3 %collective-permute-done.6 = bf16[512,2,64]{0,2,1:T(8,128)(2,1)S(1)} collective-permute-done((bf16[512,2,64]{0,2,1:T(8,128)(2,1)S(1)}, bf16[512,2,64]{0,2,1:T(8,128)(2,1)S(1)}, u32[]{:S(2)}, u32[]{:S(2)}) %collective-permute-start.6) | collective-permute-done | bytes 131104 | tf_op jit(solution)/shard_map/ppermute | solution.py:78
  68.8 38.0 %while.13 = (s32[]{:T(128)}, f32[512,2,2,64]{0,3,2,1:T(8,128)S(1)}, f32[512,2,2]{0,2,1:T(2,128)S(1)}, bf16[4,1024,2,64]{1,3,2,0:T(8,128)(2,1)S(1)}, bf16[4,1024,...) while((s32[]{:T(128)}, f32[512,2,2,64]{0,3,2,1:T(8,128)S(1)}, ...), condition=%wide.region_4.5_spmd.clone, body=%wide.region_2.4_spmd.clone.sunk | while | flops 545523712 | bytes 18645096 | solution.py:106
  68.9 4.6 %bitcast_reduce_fusion.2 = (f32[512,2,2]{0,2,1:T(2,128)S(1)}, f32[2,1024,512,2]{2,1,3,0:T(8,128)}) fusion(bf16[512,2,2,64]{0,3,2,1:T(8,128)(2,1)S(1)} %get-tuple-element.193, bf16[4,1024,2,64]{1,3,2,0:T(8,128)(2,1)S(1)} %get-tuple-element.192, s32[]{:T(128)} %get-tuple-element.180), kind=kOutput, calls=%fused_computation.1.clone.1 | convolution fusion | flops 272627712 | bytes 8921092 | tf_op jit(solution)/shard_map/while/body/eval_jaxpr/thgd,nhd->thgn/dot_general | solution.py:91
  73.5 4.9 %fusion.58 = f32[512,2,2,64]{0,3,2,1:T(8,128)S(1)} fusion(f32[2,1024,512,2]{2,1,3,0:T(8,128)} %get-tuple-element.170, f32[512,2,2,64]{0,3,2,1:T(8,128)S(1)} %get-tuple-element.181, bf16[4,1024,2,64]{1,3,2,0:T(8,128)(2,1)S(1)} %get-tuple-element.191, s32[]{:T(128)} %get-tuple-element.180, pred[]{:T(512)S(6)} %compare.15), kind=kOutput, calls=%fused_computation.7.clone.1 | convolution fusion | flops 272891904 | bytes 9699333 | tf_op jit(solution)/shard_map/while/body/eval_jaxpr/thgn,nhd->thgd/dot_general | solution.py:98
  78.4 4.6 %bitcast_reduce_fusion.2 = (f32[512,2,2]{0,2,1:T(2,128)S(1)}, f32[2,1024,512,2]{2,1,3,0:T(8,128)}) fusion(bf16[512,2,2,64]{0,3,2,1:T(8,128)(2,1)S(1)} %get-tuple-element.193, bf16[4,1024,2,64]{1,3,2,0:T(8,128)(2,1)S(1)} %get-tuple-element.192, s32[]{:T(128)} %get-tuple-element.180), kind=kOutput, calls=%fused_computation.1.clone.1 | convolution fusion | flops 272627712 | bytes 8921092 | tf_op jit(solution)/shard_map/while/body/eval_jaxpr/thgd,nhd->thgn/dot_general | solution.py:91
  83.0 4.9 %fusion.58 = f32[512,2,2,64]{0,3,2,1:T(8,128)S(1)} fusion(f32[2,1024,512,2]{2,1,3,0:T(8,128)} %get-tuple-element.170, f32[512,2,2,64]{0,3,2,1:T(8,128)S(1)} %get-tuple-element.181, bf16[4,1024,2,64]{1,3,2,0:T(8,128)(2,1)S(1)} %get-tuple-element.191, s32[]{:T(128)} %get-tuple-element.180, pred[]{:T(512)S(6)} %compare.15), kind=kOutput, calls=%fused_computation.7.clone.1 | convolution fusion | flops 272891904 | bytes 9699333 | tf_op jit(solution)/shard_map/while/body/eval_jaxpr/thgn,nhd->thgd/dot_general | solution.py:98
  87.9 4.6 %bitcast_reduce_fusion.2 = (f32[512,2,2]{0,2,1:T(2,128)S(1)}, f32[2,1024,512,2]{2,1,3,0:T(8,128)}) fusion(bf16[512,2,2,64]{0,3,2,1:T(8,128)(2,1)S(1)} %get-tuple-element.193, bf16[4,1024,2,64]{1,3,2,0:T(8,128)(2,1)S(1)} %get-tuple-element.192, s32[]{:T(128)} %get-tuple-element.180), kind=kOutput, calls=%fused_computation.1.clone.1 | convolution fusion | flops 272627712 | bytes 8921092 | tf_op jit(solution)/shard_map/while/body/eval_jaxpr/thgd,nhd->thgn/dot_general | solution.py:91
  92.5 4.9 %fusion.58 = f32[512,2,2,64]{0,3,2,1:T(8,128)S(1)} fusion(f32[2,1024,512,2]{2,1,3,0:T(8,128)} %get-tuple-element.170, f32[512,2,2,64]{0,3,2,1:T(8,128)S(1)} %get-tuple-element.181, bf16[4,1024,2,64]{1,3,2,0:T(8,128)(2,1)S(1)} %get-tuple-element.191, s32[]{:T(128)} %get-tuple-element.180, pred[]{:T(512)S(6)} %compare.15), kind=kOutput, calls=%fused_computation.7.clone.1 | convolution fusion | flops 272891904 | bytes 9699333 | tf_op jit(solution)/shard_map/while/body/eval_jaxpr/thgn,nhd->thgd/dot_general | solution.py:98
  97.4 4.6 %bitcast_reduce_fusion.2 = (f32[512,2,2]{0,2,1:T(2,128)S(1)}, f32[2,1024,512,2]{2,1,3,0:T(8,128)}) fusion(bf16[512,2,2,64]{0,3,2,1:T(8,128)(2,1)S(1)} %get-tuple-element.193, bf16[4,1024,2,64]{1,3,2,0:T(8,128)(2,1)S(1)} %get-tuple-element.192, s32[]{:T(128)} %get-tuple-element.180), kind=kOutput, calls=%fused_computation.1.clone.1 | convolution fusion | flops 272627712 | bytes 8921092 | tf_op jit(solution)/shard_map/while/body/eval_jaxpr/thgd,nhd->thgn/dot_general | solution.py:91
  102.0 4.9 %fusion.58 = f32[512,2,2,64]{0,3,2,1:T(8,128)S(1)} fusion(f32[2,1024,512,2]{2,1,3,0:T(8,128)} %get-tuple-element.170, f32[512,2,2,64]{0,3,2,1:T(8,128)S(1)} %get-tuple-element.181, bf16[4,1024,2,64]{1,3,2,0:T(8,128)(2,1)S(1)} %get-tuple-element.191, s32[]{:T(128)} %get-tuple-element.180, pred[]{:T(512)S(6)} %compare.15), kind=kOutput, calls=%fused_computation.7.clone.1 | convolution fusion | flops 272891904 | bytes 9699333 | tf_op jit(solution)/shard_map/while/body/eval_jaxpr/thgn,nhd->thgd/dot_general | solution.py:98
  107.8 3.4 %all-to-all-start = ((bf16[4,128,256]{1,2,0:T(8,128)(2,1)}), bf16[4,128,256]{1,2,0:T(8,128)(2,1)S(1)}, u32[]{:S(2)}, u32[]{:S(2)}) async-start(bf16[4,128,256]{1,2,0:T(8,128)(2,1)} %copy.76), calls=%async_computation | async-start | bytes 524288 | tf_op jit(solution)/shard_map/all_to_all | solution.py:111
  111.3 5.9 %all-to-all-done = bf16[4,128,256]{1,2,0:T(8,128)(2,1)S(1)} async-done(((bf16[4,128,256]{1,2,0:T(8,128)(2,1)}), bf16[4,128,256]{1,2,0:T(8,128)(2,1)S(1)}, u32[]{:S(2)}, u32[]{:S(2)}) %all-to-all-start) | async-done | bytes 262176 | tf_op jit(solution)/shard_map/all_to_all | solution.py:111
  121.7 50.7 %all_to_all.29 = bf16[32,16,2048]{2,1,0:T(8,128)(2,1)S(1)} all-to-all(bf16[32,16,2048]{2,1,0:T(8,128)(2,1)S(1)} %bitcast.113), channel_id=1, replica_groups=mesh['sp'=8,'tp'=4] {'sp','tp'}, dimensions={0} | all-to-all | bytes 4194304 | tf_op jit(solution)/shard_map/all_to_all | solution.py:137
  172.4 3.7 %fusion.16 = f32[512,1024]{1,0:T(8,128)} fusion(bf16[512,2048]{1,0:T(8,128)(2,1)S(1)} %bitcast.118, bf16[1,2048,1024]{2,1,0:T(8,128)(2,1)S(1)} %copy-done.6), kind=kOutput, calls=%fused_computation.21 | convolution fusion | flops 2147483648 | bytes 8388608 | tf_op jit(solution)/shard_map/dot_general | solution.py:139
  176.1 9.9 %fusion.18 = bf16[512,2048]{1,0:T(8,128)(2,1)} fusion(bf16[1,1024,2048]{2,1,0:T(8,128)(2,1)} %param.25, f32[512,1024]{1,0:T(8,128)} %fusion.16, bf16[512,2048]{1,0:T(8,128)(2,1)S(1)} %bitcast.119, bf16[1,2048,1024]{2,1,0:T(8,128)(2,1)} %param.24), kind=kOutput, calls=%fused_computation.23 | convolution fusion | flops 4299161600 | bytes 14680064 | tf_op jit(solution)/shard_map/dot_general | solution.py:142
  186.0 3.6 %all-to-all-start.2 = ((bf16[32,16,2048]{2,1,0:T(8,128)(2,1)}), bf16[32,16,2048]{2,1,0:T(8,128)(2,1)S(1)}, u32[]{:S(2)}, u32[]{:S(2)}) async-start(bf16[32,16,2048]{2,1,0:T(8,128)(2,1)} %bitcast.117), calls=%async_computation.2 | async-start | bytes 4194304 | tf_op jit(solution)/shard_map/all_to_all | solution.py:144
  190.2 48.2 %all-to-all-done.2 = bf16[32,16,2048]{2,1,0:T(8,128)(2,1)S(1)} async-done(((bf16[32,16,2048]{2,1,0:T(8,128)(2,1)}), bf16[32,16,2048]{2,1,0:T(8,128)(2,1)S(1)}, u32[]{:S(2)}, u32[]{:S(2)}) %all-to-all-start.2) | async-done | bytes 2097184 | tf_op jit(solution)/shard_map/all_to_all | solution.py:144
  242.4 4.1 %multiply_reduce_fusion = f32[128,2048]{1,0:T(8,128)S(1)} fusion(bf16[128,2,2048]{2,1,0:T(2,128)(2,1)S(1)} %gather.7, pred[128,2]{1,0:T(8,128)(4,1)S(1)} %copy.81, f32[128,2]{1,0:T(8,128)S(1)} %copy.83), kind=kLoop, calls=%fused_computation.25 | loop fusion | flops 1835008 | bytes 2098432 | tf_op jit(solution)/shard_map/reduce_sum | solution.py:148
  (96 shorter events, 21.3 us)
Async XLA Ops:
  6.5 6.3 %copy-start.2 = (s32[128,2]{0,1:T(2,128)S(1)}, s32[128,2]{0,1:T(2,128)}, u32[]{:S(2)}) copy-start(s32[128,2]{0,1:T(2,128)} %param.21) | copy-start | bytes 3076
  6.5 19.2 %copy-start.1 = (bf16[512,256]{1,0:T(8,128)(2,1)S(1)}, bf16[512,256]{1,0:T(8,128)(2,1)}, u32[]{:S(2)}) copy-start(bf16[512,256]{1,0:T(8,128)(2,1)} %param.14) | copy-start | bytes 786436
  6.5 61.0 %all-gather.2.cloned.1.call-start = ((), (), s32[]{:S(2)}) async-start(), calls=%async_computation.3 | async-start | bytes 1179648 | tf_op jit(solution)/shard_map/all_gather | solution.py:82
  8.1 9.6 %collective-permute-start = (bf16[512,2,64]{0,2,1:T(8,128)(2,1)S(1)}, bf16[512,2,64]{0,2,1:T(8,128)(2,1)S(1)}, u32[]{:S(2)}, u32[]{:S(2)}) collective-permute-start(bf16[512,2,64]{0,2,1:T(8,128)(2,1)S(1)} %pad_maximum_fusion.1), channel_id=1, source_target_pairs={{0,4},{4,8},{8,12},{12,16},{16,20},{20,24},{24,28},{28,0},{1,5},{5... | collective-permute-start | bytes 393224 | tf_op jit(solution)/shard_map/ppermute | solution.py:78
  17.7 7.8 %collective-permute-start.1 = (bf16[512,2,64]{0,2,1:T(8,128)(2,1)S(1)}, bf16[512,2,64]{0,2,1:T(8,128)(2,1)S(1)}, u32[]{:S(2)}, u32[]{:S(2)}) collective-permute-start(bf16[512,2,64]{0,2,1:T(8,128)(2,1)S(1)} %collective-permute-done), channel_id=1, source_target_pairs={{0,4},{4,8},{8,12},{12,16},{16,20},{20,24},{24,28},{28,0},{1,5},{5... | collective-permute-start | bytes 393224 | tf_op jit(solution)/shard_map/ppermute | solution.py:78
  25.4 8.4 %collective-permute-start.2 = (bf16[512,2,64]{0,2,1:T(8,128)(2,1)S(1)}, bf16[512,2,64]{0,2,1:T(8,128)(2,1)S(1)}, u32[]{:S(2)}, u32[]{:S(2)}) collective-permute-start(bf16[512,2,64]{0,2,1:T(8,128)(2,1)S(1)} %collective-permute-done.1), channel_id=1, source_target_pairs={{0,4},{4,8},{8,12},{12,16},{16,20},{20,24},{24,28},{28,0},{1,5},{5... | collective-permute-start | bytes 393224 | tf_op jit(solution)/shard_map/ppermute | solution.py:78
  33.8 7.7 %collective-permute-start.3 = (bf16[512,2,64]{0,2,1:T(8,128)(2,1)S(1)}, bf16[512,2,64]{0,2,1:T(8,128)(2,1)S(1)}, u32[]{:S(2)}, u32[]{:S(2)}) collective-permute-start(bf16[512,2,64]{0,2,1:T(8,128)(2,1)S(1)} %collective-permute-done.2), channel_id=1, source_target_pairs={{0,4},{4,8},{8,12},{12,16},{16,20},{20,24},{24,28},{28,0},{1,5},{5... | collective-permute-start | bytes 393224 | tf_op jit(solution)/shard_map/ppermute | solution.py:78
  41.5 8.2 %collective-permute-start.4 = (bf16[512,2,64]{0,2,1:T(8,128)(2,1)S(1)}, bf16[512,2,64]{0,2,1:T(8,128)(2,1)S(1)}, u32[]{:S(2)}, u32[]{:S(2)}) collective-permute-start(bf16[512,2,64]{0,2,1:T(8,128)(2,1)S(1)} %collective-permute-done.3), channel_id=1, source_target_pairs={{0,4},{4,8},{8,12},{12,16},{16,20},{20,24},{24,28},{28,0},{1,5},{5... | collective-permute-start | bytes 393224 | tf_op jit(solution)/shard_map/ppermute | solution.py:78
  49.6 9.7 %collective-permute-start.5 = (bf16[512,2,64]{0,2,1:T(8,128)(2,1)S(1)}, bf16[512,2,64]{0,2,1:T(8,128)(2,1)S(1)}, u32[]{:S(2)}, u32[]{:S(2)}) collective-permute-start(bf16[512,2,64]{0,2,1:T(8,128)(2,1)S(1)} %collective-permute-done.4), channel_id=1, source_target_pairs={{0,4},{4,8},{8,12},{12,16},{16,20},{20,24},{24,28},{28,0},{1,5},{5... | collective-permute-start | bytes 393224 | tf_op jit(solution)/shard_map/ppermute | solution.py:78
  59.4 7.7 %collective-permute-start.6 = (bf16[512,2,64]{0,2,1:T(8,128)(2,1)S(1)}, bf16[512,2,64]{0,2,1:T(8,128)(2,1)S(1)}, u32[]{:S(2)}, u32[]{:S(2)}) collective-permute-start(bf16[512,2,64]{0,2,1:T(8,128)(2,1)S(1)} %collective-permute-done.5), channel_id=1, source_target_pairs={{0,4},{4,8},{8,12},{12,16},{16,20},{20,24},{24,28},{28,0},{1,5},{5... | collective-permute-start | bytes 393224 | tf_op jit(solution)/shard_map/ppermute | solution.py:78
  107.8 9.4 %all-to-all-start = ((bf16[4,128,256]{1,2,0:T(8,128)(2,1)}), bf16[4,128,256]{1,2,0:T(8,128)(2,1)S(1)}, u32[]{:S(2)}, u32[]{:S(2)}) async-start(bf16[4,128,256]{1,2,0:T(8,128)(2,1)} %copy.76), calls=%async_computation | async-start | bytes 524288 | tf_op jit(solution)/shard_map/all_to_all | solution.py:111
  117.1 3.1 %copy-start = (bf16[128,2048]{1,0:T(8,128)(2,1)S(1)}, bf16[128,2048]{1,0:T(8,128)(2,1)}, u32[]{:S(2)}) copy-start(bf16[128,2048]{1,0:T(8,128)(2,1)} %param.17) | copy-start | bytes 1572868
  117.1 3.1 %copy-start.3 = (f32[2048]{0:T(1024)S(1)}, f32[2048]{0:T(1024)}, u32[]{:S(2)}) copy-start(f32[2048]{0:T(1024)} %param.19) | copy-start | bytes 24580
  120.2 0.7 copy-start.4
  121.7 50.7 %copy-start.6 = (bf16[1,2048,1024]{2,1,0:T(8,128)(2,1)S(1)}, bf16[1,2048,1024]{2,1,0:T(8,128)(2,1)}, u32[]{:S(2)}) copy-start(bf16[1,2048,1024]{2,1,0:T(8,128)(2,1)} %param.23) | copy-start | bytes 12582916
  186.0 4.0 %copy-start.5 = (f32[128,2]{0,1:T(2,128)S(1)}, f32[128,2]{0,1:T(2,128)}, u32[]{:S(2)}) copy-start(f32[128,2]{0,1:T(2,128)} %param.22) | copy-start | bytes 3076
  186.0 52.3 %all-to-all-start.2 = ((bf16[32,16,2048]{2,1,0:T(8,128)(2,1)}), bf16[32,16,2048]{2,1,0:T(8,128)(2,1)S(1)}, u32[]{:S(2)}, u32[]{:S(2)}) async-start(bf16[32,16,2048]{2,1,0:T(8,128)(2,1)} %bitcast.117), calls=%async_computation.2 | async-start | bytes 4194304 | tf_op jit(solution)/shard_map/all_to_all | solution.py:144
Sparse Core Ops, SparseCore 0:
  12.9 42.3 all-gather.1
